TPU v7x, 32 devices: a whole 2x2x4 slice. The times are simulated.
32 devices in a mesh: fs: 8 (over z, x), tp: 4 (over y, core).
Axes of the slice: x: 2, y: 2, z: 4, core: 2. Of those that a mesh axis runs over, the one named last changes fastest.
Arguments:
- later_rows: bfloat16 [4096, 2048], P(('fs', 'tp')), may hold values from -6 to 6
- earlier_rows: bfloat16 [4096, 2048], P(('fs', 'tp')), may hold values from -6 to 6
- cotangent: bfloat16 [4096, 2048], P(('fs', 'tp')), may hold values from -6 to 6
- up_weight: bfloat16 [2048, 4096], P('fs', 'tp'), may hold values from -0.125 to 0.125
- down_weight: bfloat16 [2048, 4096], P('fs', 'tp'), may hold values from -0.09375 to 0.09375
- up_total: float32 [2048, 4096], P('fs', 'tp'), may hold values from -6 to 6
- down_total: float32 [2048, 4096], P('fs', 'tp'), may hold values from -6 to 6
Outputs:
- later_out: bfloat16 [4096, 2048], P(('fs', 'tp'))
- earlier_grad: bfloat16 [4096, 2048], P(('fs', 'tp'))
- up_updated: float32 [2048, 4096], P('fs', 'tp')
- down_updated: float32 [2048, 4096], P('fs', 'tp')
All inputs are finite; a program needn't handle non-finite values.
Results may differ from a plain program's by a relative error of at most 0.015.
Values may be sent and summed in bfloat16 or wider, within the bound.
A program may use at most 128 MiB of HBM per device.

v0:
```python
import math

import jax
import jax.numpy as jnp
from jax import lax
from jax.sharding import PartitionSpec as P


def contract_last(left, right):
    return lax.dot_general(
        left, right, (((1,), (1,)), ((), ())), preferred_element_type=jnp.float32
    )


def body(later_rows, earlier_rows, cotangent, up_weight, down_weight, up_total, down_total):
    rows_dev = later_rows.shape[0]
    total_rows = rows_dev * lax.axis_size("fs") * lax.axis_size("tp")
    factor = 1.0 / math.sqrt(total_rows)
    up_full, down_full = (
        lax.all_gather(up_weight, "fs", axis=0, tiled=True),
        lax.all_gather(down_weight, "fs", axis=0, tiled=True),
    )

    def fetch():
        return (up_full, down_full)

    def to_owner(term):
        return lax.psum_scatter(
            term.astype(jnp.bfloat16), "tp", scatter_dimension=0, tiled=True
        ).astype(jnp.float32)

    def grad_owner(group, right):
        return lax.psum_scatter(
            lax.dot_general(
                group, right, (((0,), (0,)), ((), ())), preferred_element_type=jnp.float32
            ).astype(jnp.bfloat16),
            "fs",
            scatter_dimension=0,
            tiled=True,
        ).astype(jnp.float32)

    up_whole, down_whole = fetch()
    group = lax.all_gather(later_rows, "tp", axis=0, tiled=True)
    relu_part = jnp.maximum(jnp.dot(group, up_whole, preferred_element_type=jnp.float32), 0.0)
    hidden = (relu_part * relu_part).astype(jnp.bfloat16)
    partial_value = contract_last(hidden, down_whole)
    later_out = to_owner(partial_value).astype(jnp.bfloat16)
    up_whole, down_whole = fetch()
    saved_group = lax.all_gather(earlier_rows, "tp", axis=0, tiled=True)
    cot_group = lax.all_gather(cotangent, "tp", axis=0, tiled=True)
    relu_part = jnp.maximum(jnp.dot(saved_group, up_whole, preferred_element_type=jnp.float32), 0.0)
    hidden = (relu_part * relu_part).astype(jnp.bfloat16)
    hidden_grad = jnp.dot(cot_group, down_whole, preferred_element_type=jnp.float32)
    pre_grad = (2.0 * relu_part * hidden_grad).astype(jnp.bfloat16)
    input_partial = contract_last(pre_grad, up_whole)
    earlier_grad = to_owner(input_partial).astype(jnp.bfloat16)
    down_updated = down_total + grad_owner(cot_group, hidden) * factor
    up_updated = up_total + grad_owner(saved_group, pre_grad) * factor
    earlier_grad, up_updated, down_updated = (earlier_grad, up_updated, down_updated)
    return (later_out, earlier_grad, up_updated, down_updated)


def solution(mesh):
    return jax.shard_map(
        body,
        mesh=mesh,
        in_specs=(
            P(("fs", "tp"), None),
            P(("fs", "tp"), None),
            P(("fs", "tp"), None),
            P("fs", "tp"),
            P("fs", "tp"),
            P("fs", "tp"),
            P("fs", "tp"),
        ),
        out_specs=(P(("fs", "tp"), None), P(("fs", "tp"), None), P("fs", "tp"), P("fs", "tp")),
        check_vma=False,
    )
```

profile of v0, /device:TPU:0, one launch (start us, length us, event | category | flops | bytes accessed | tf_op | source)
XLA Modules:
  0.0 488.9 jit_solution(10079960880024207765)
XLA Ops:
  7.2 0.0 all-gather.12.cloned.1.call-start
  7.2 0.7 all-gather.12.cloned.1.call-update
  7.9 0.0 all-gather.8.cloned.1.call-start
  7.9 0.7 all-gather.8.cloned.1.call-update
  8.6 0.0 all-gather.14.cloned.1.call-start
  8.7 0.7 all-gather.14.cloned.1.call-update
  9.4 0.0 all-gather.10.cloned.1.call-start
  9.4 0.5 all-gather.10.cloned.1.call-update
  10.0 0.0 all-gather.6.cloned.1.call-start
  10.0 0.5 all-gather.6.cloned.1.call-update
  10.5 0.0 reduce-scatter.9.cloned.1.call-start
  10.6 24.3 %all-gather.12.cloned.1.call-done = bf16[512,2048]{1,0:T(8,128)(2,1)} async-done(((bf16[128,2048]{1,0:T(8,128)(2,1)}), bf16[512,2048]{1,0:T(8,128)(2,1)}) %all-gather.12.cloned.1.call-update) | async-done | bytes 2097168 | tf_op jit(solution)/shard_map/all_gather | solution.py:49
  34.9 74.9 %all-gather.8.cloned.1.call-done = bf16[2048,1024]{1,0:T(8,128)(2,1)} async-done(((bf16[256,1024]{1,0:T(8,128)(2,1)}), bf16[2048,1024]{1,0:T(8,128)(2,1)}) %all-gather.8.cloned.1.call-update) | async-done | bytes 4194320 | tf_op jit(solution)/shard_map/all_gather | solution.py:20
  109.8 6.5 %fusion.3 = f32[512,1024]{1,0:T(8,128)} fusion(bf16[512,2048]{1,0:T(8,128)(2,1)} %all-gather.12.cloned.1.call-done, bf16[2048,1024]{1,0:T(8,128)(2,1)} %all-gather.8.cloned.1.call-done), kind=kOutput, calls=%fused_computation.12 | convolution fusion | flops 2147483648 | bytes 8388608 | tf_op jit(solution)/shard_map/dot_general | solution.py:51
  116.3 0.0 copy-start.2
  116.3 16.2 %all-gather.14.cloned.1.call-done = bf16[512,2048]{1,0:T(8,128)(2,1)} async-done(((bf16[128,2048]{1,0:T(8,128)(2,1)}), bf16[512,2048]{1,0:T(8,128)(2,1)}) %all-gather.14.cloned.1.call-update) | async-done | bytes 2097168 | tf_op jit(solution)/shard_map/all_gather | solution.py:50
  132.5 74.8 %all-gather.10.cloned.1.call-done = bf16[2048,1024]{1,0:T(8,128)(2,1)} async-done(((bf16[256,1024]{1,0:T(8,128)(2,1)}), bf16[2048,1024]{1,0:T(8,128)(2,1)}) %all-gather.10.cloned.1.call-update) | async-done | bytes 4194320 | tf_op jit(solution)/shard_map/all_gather | solution.py:21
  207.3 5.8 %multiply_convert_fusion.1 = bf16[512,1024]{1,0:T(8,128)(2,1)S(1)} fusion(f32[512,1024]{1,0:T(8,128)} %fusion.3, bf16[512,2048]{1,0:T(8,128)(2,1)} %all-gather.14.cloned.1.call-done, bf16[2048,1024]{1,0:T(8,128)(2,1)} %all-gather.10.cloned.1.call-done), kind=kOutput, calls=%fused_computation.5 | convolution fusion | flops 2149580800 | bytes 9437184 | tf_op jit(solution)/shard_map/dot_general | solution.py:53
  213.1 0.0 copy-done.2
  213.1 4.4 convert_bitcast_fusion.1
  217.5 0.0 copy-start.3
  217.5 0.0 reduce-scatter.9.cloned.1.call-update
  217.5 0.0 reduce-scatter.11.cloned.1.call-start
  217.6 1.5 copy-done.3
  219.1 5.9 %convert_bitcast_fusion = bf16[2048,1024]{0,1:T(8,128)(2,1)} fusion(bf16[512,2048]{1,0:T(8,128)(2,1)S(1)} %copy-done.3, f32[512,1024]{1,0:T(8,128)} %fusion.3), kind=kOutput, calls=%fused_computation | convolution fusion | flops 2151153664 | bytes 8388608 | tf_op jit(solution)/shard_map/dot_general | solution.py:34
  225.0 0.0 reduce-scatter.11.cloned.1.call-update
  225.0 0.0 reduce-scatter.5.cloned.1.call-start
  225.1 4.8 all-gather.6.cloned.1.call-done
  229.8 9.9 %convolution_convert_fusion.1 = bf16[512,2048]{1,0:T(8,128)(2,1)} fusion(bf16[2048,1024]{1,0:T(8,128)(2,1)} %all-gather.10.cloned.1.call-done, bf16[512,2048]{1,0:T(8,128)(2,1)} %all-gather.6.cloned.1.call-done, bf16[2048,1024]{1,0:T(8,128)(2,1)} %all-gather.8.cloned.1.call-done), kind=kOutput, calls=%fused_computation.3 | convolution fusion | flops 4297588736 | bytes 12582912 | tf_op jit(solution)/shard_map/dot_general | solution.py:10
  239.7 0.0 reduce-scatter.5.cloned.1.call-update
  239.8 0.2 reduce-scatter.7.cloned.1.call-start
  240.0 6.0 %convolution_convert_fusion = bf16[512,2048]{1,0:T(8,128)(2,1)} fusion(bf16[512,1024]{1,0:T(8,128)(2,1)S(1)} %multiply_convert_fusion.1, bf16[2048,1024]{1,0:T(8,128)(2,1)} %all-gather.8.cloned.1.call-done), kind=kOutput, calls=%fused_computation.2 | convolution fusion | flops 2148532224 | bytes 7340032 | tf_op jit(solution)/shard_map/dot_general | solution.py:10
  246.0 0.0 copy-start
  246.0 0.0 copy-start.1
  246.0 0.0 reduce-scatter.7.cloned.1.call-update
  246.1 1.2 copy-done
  247.3 0.3 copy.11
  247.6 0.0 copy-done.1
  247.6 0.3 copy.12
  248.0 74.2 %reduce-scatter.9.cloned.1.call-done = bf16[256,1024]{0,1:T(8,128)(2,1)} async-done(((bf16[2048,1024]{0,1:T(8,128)(2,1)}), bf16[256,1024]{0,1:T(8,128)(2,1)}) %reduce-scatter.9.cloned.1.call-update) | async-done | bytes 524304 | tf_op jit(solution)/shard_map/reduce_scatter | solution.py:33
  322.1 1.1 multiply_add_fusion.1
  323.3 1.3 copy.13
  324.6 89.5 %reduce-scatter.11.cloned.1.call-done = bf16[256,1024]{0,1:T(8,128)(2,1)} async-done(((bf16[2048,1024]{0,1:T(8,128)(2,1)}), bf16[256,1024]{0,1:T(8,128)(2,1)}) %reduce-scatter.11.cloned.1.call-update) | async-done | bytes 524304 | tf_op jit(solution)/shard_map/reduce_scatter | solution.py:33
  414.1 1.1 multiply_add_fusion
  415.2 1.3 copy.14
  416.5 31.5 %reduce-scatter.5.cloned.1.call-done = bf16[128,2048]{1,0:T(8,128)(2,1)} async-done(((bf16[512,2048]{1,0:T(8,128)(2,1)}), bf16[128,2048]{1,0:T(8,128)(2,1)}) %reduce-scatter.5.cloned.1.call-update) | async-done | bytes 524304 | tf_op jit(solution)/shard_map/reduce_scatter | solution.py:28
  448.0 34.3 %reduce-scatter.7.cloned.1.call-done = bf16[128,2048]{1,0:T(8,128)(2,1)} async-done(((bf16[512,2048]{1,0:T(8,128)(2,1)}), bf16[128,2048]{1,0:T(8,128)(2,1)}) %reduce-scatter.7.cloned.1.call-update) | async-done | bytes 524304 | tf_op jit(solution)/shard_map/reduce_scatter | solution.py:28
Async XLA Ops:
  7.2 27.7 %all-gather.12.cloned.1.call-start = ((), (), s32[]{:S(2)}) async-start(), calls=%async_computation.8 | async-start | bytes 2621440 | tf_op jit(solution)/shard_map/all_gather | solution.py:49
  7.9 101.9 %all-gather.8.cloned.1.call-start = ((), (), s32[]{:S(2)}) async-start(), calls=%async_computation.5 | async-start | bytes 4718592 | tf_op jit(solution)/shard_map/all_gather | solution.py:20
  8.6 123.8 %all-gather.14.cloned.1.call-start = ((), (), s32[]{:S(2)}) async-start(), calls=%async_computation.9 | async-start | bytes 2621440 | tf_op jit(solution)/shard_map/all_gather | solution.py:50
  9.4 197.9 %all-gather.10.cloned.1.call-start = ((), (), s32[]{:S(2)}) async-start(), calls=%async_computation.6 | async-start | bytes 4718592 | tf_op jit(solution)/shard_map/all_gather | solution.py:21
  10.0 219.9 %all-gather.6.cloned.1.call-start = ((), (), s32[]{:S(2)}) async-start(), calls=%async_computation.4 | async-start | bytes 2621440 | tf_op jit(solution)/shard_map/all_gather | solution.py:43
  10.5 311.6 %reduce-scatter.9.cloned.1.call-start = ((), (), s32[]{:S(2)}) async-start(), calls=%async_computation.11 | async-start | bytes 4718592 | tf_op jit(solution)/shard_map/reduce_scatter | solution.py:33
  116.3 96.8 %copy-start.2 = (bf16[512,2048]{1,0:T(8,128)(2,1)S(1)}, bf16[512,2048]{1,0:T(8,128)(2,1)}, u32[]{:S(2)}) copy-start(bf16[512,2048]{1,0:T(8,128)(2,1)} %all-gather.12.cloned.1.call-done) | copy-start | bytes 6291460
  217.5 1.6 copy-start.3
  217.5 196.6 %reduce-scatter.11.cloned.1.call-start = ((), (), s32[]{:S(2)}) async-start(), calls=%async_computation.12 | async-start | bytes 4718592 | tf_op jit(solution)/shard_map/reduce_scatter | solution.py:33
  225.0 223.0 %reduce-scatter.5.cloned.1.call-start = ((), (), s32[]{:S(2)}) async-start(), calls=%async_computation.7 | async-start | bytes 2621440 | tf_op jit(solution)/shard_map/reduce_scatter | solution.py:28
  239.8 242.6 %reduce-scatter.7.cloned.1.call-start = ((), (), s32[]{:S(2)}) async-start(), calls=%async_computation.10 | async-start | bytes 2621440 | tf_op jit(solution)/shard_map/reduce_scatter | solution.py:28
  246.0 1.2 copy-start
  246.0 1.6 copy-start.1
Sparse Core Ops, SparseCore 0:
  9.5 25.2 all-gather.11
  37.0 72.7 all-gather.7
  111.4 21.0 all-gather.13
  134.5 72.7 all-gather.9
  208.7 21.0 all-gather.5
  233.3 88.7 reduce-scatter.8
  325.7 88.3 reduce-scatter.10
  417.2 30.8 reduce-scatter.4
  451.1 31.1 reduce-scatter.6
where the time goes:
time: 489 us
  waiting for transfers between devices  428 us (88%)
  matrix products  38.5 us (8%)
  between operations  13.9 us (3%)
  local copies, waits for them, and re-layouts  6.01 us (1%)
    reduce_scatter x2, waiting for transfers between devices, grad_owner(): lax.psum_scatter(lax.dot_general(group, right, (((0,), (0,)), ((), ())),...  164 us
    all_gather x1, waiting for transfers between devices, body(): lax.all_gather(up_weight, 'fs', axis=0, tiled=True)  74.9 us
    all_gather x1, waiting for transfers between devices, body(): lax.all_gather(down_weight, 'fs', axis=0, tiled=True)  74.8 us
    reduce_scatter x2, waiting for transfers between devices, to_owner(): lax.psum_scatter(term.astype(jnp.bfloat16), 'tp', scatter_dimension=0, ti...  65.8 us
    all_gather x1, waiting for transfers between devices, body(): saved_group = lax.all_gather(earlier_rows, 'tp', axis=0, tiled=True)  24.3 us
    all_gather x1, waiting for transfers between devices, body(): cot_group = lax.all_gather(cotangent, 'tp', axis=0, tiled=True)  16.2 us
    dot_general x2, matrix products, contract_last(): lax.dot_general(left, right, (((1,), (1,)), ((), ())), preferred_element_...  15.9 us
    dot_general x2, matrix products, grad_owner(): lax.dot_general(group, right, (((0,), (0,)), ((), ())), preferred_element...  10.3 us
  transfers between devices with their start and end apart: 9, of which 9 were waited for; matrix products, arithmetic and copies ran while one was open for 9% of the time, Pallas kernels for 0%

commit v1 on v0

v1 whole, which is shorter than its diff:
```python
import functools
import math

import jax
import jax.numpy as jnp
from jax import lax
from jax.experimental import pallas as pl
from jax.experimental.pallas import tpu as pltpu
from jax.sharding import PartitionSpec as P

MESH = pl.DeviceIdType.MESH
BF16 = jnp.bfloat16
F32 = jnp.float32


def columns_of(n):
    best = 1
    for x in range(1, n + 1):
        if n % x == 0 and 2 * x * x <= n and (n // x) % 2 == 0:
            best = x
    return best


def ring_to_fs(p, n, x_size):
    if x_size == 1:
        return p
    z_size, wide = n // x_size, x_size - 1
    body = z_size * wide
    z, r = p // wide, p % wide
    x = 1 + jnp.where(z % 2 == 0, r, wide - 1 - r)
    back = z_size - 1 - (p - body)
    return jnp.where(p < body, z * x_size + x, back * x_size)


def fs_to_ring(f, n, x_size):
    if x_size == 1:
        return f
    z_size, wide = n // x_size, x_size - 1
    z, x = f // x_size, f % x_size
    r = jnp.where(z % 2 == 0, x - 1, x_size - 1 - x)
    return jnp.where(x == 0, z_size * wide + z_size - 1 - z, z * wide + r)


def kernel(n, m, factor,
           later_ref, earlier_ref, cot_ref, up_ref, down_ref, up_tot_ref, down_tot_ref,
           later_out, earlier_out, up_out, down_out,
           tok, wts, acc, hid, grads, rbuf, part, dbuf, ybuf,
           ty_s, ty_r, td_s, td_r, w_s, w_r, g_s, g_r, od_s, od_r, oy_s, oy_r):
    rows_dev, depth = later_ref.shape
    blk, width = up_ref.shape
    rows = rows_dev * m
    half, y_size = n // 2, m // 2
    aligned = blk % 128 == 0
    fs, tp = lax.axis_index("fs"), lax.axis_index("tp")
    x_size = columns_of(n)
    pos = fs_to_ring(fs, n, x_size)
    y, c = tp // 2, tp % 2

    def at_ring(p):
        return ring_to_fs((p + 2 * n) % n, n, x_size)

    right = {"fs": at_ring(pos + 1), "tp": tp}
    left = {"fs": at_ring(pos - 1), "tp": tp}
    mate = {"fs": fs, "tp": y * 2 + 1 - c}
    y_next = {"fs": fs, "tp": ((y + 1) % y_size) * 2 + c}
    y_prev = {"fs": fs, "tp": ((y + y_size - 1) % y_size) * 2 + c}

    barrier = pltpu.get_barrier_semaphore()
    for other in (right, left, mate, y_next, y_prev):
        pl.semaphore_signal(barrier, inc=1, device_id=other, device_id_type=MESH)
    pl.semaphore_wait(barrier, 5)

    def remote(src, dst, send, recv, to):
        return pltpu.make_async_remote_copy(
            src_ref=src, dst_ref=dst, send_sem=send, recv_sem=recv, device_id=to, device_id_type=MESH)

    def wrows(a, f):
        return wts.at[a, pl.ds(pl.multiple_of(f * blk, blk), blk), :]

    def trows(a, t):
        return tok.at[a, pl.ds(pl.multiple_of(t * rows_dev, rows_dev), rows_dev), :]

    own_w, own_t = (up_ref, down_ref), (earlier_ref, cot_ref, later_ref)

    arr_of, sign_of = (0, 1, 1, 0), (1, -1, 1, -1)

    def w_copy(k, s, first=False):
        f = at_ring(pos - sign_of[k] * s)
        src = own_w[arr_of[k]] if first else wrows(arr_of[k], f)
        return remote(src, wrows(arr_of[k], f), w_s.at[k, s], w_r.at[k, s], right if sign_of[k] > 0 else left)

    def ty_copy(a, s, first=False):
        t = ((y + y_size - s) % y_size) * 2 + c
        return remote(own_t[a] if first else trows(a, t), trows(a, t), ty_s.at[a, s], ty_r.at[a, s], y_next)

    def td_copy(a, s, first=False):
        t = ((y + y_size - s) % y_size) * 2 + c
        return remote(own_t[a] if first else trows(a, t), trows(a, t), td_s.at[a, s], td_r.at[a, s], mate)

    for k in range(4):
        if half - (k >= 2) > 0:
            w_copy(k, 0, True).start()
    for a in range(3):
        if y_size > 1:
            ty_copy(a, 0, True).start()
    for a in range(3):
        td_copy(a, 0, True).start()

    def put(dst, dst_row, src, count):
        step = math.gcd(count, 64)

        @pl.loop(0, count // step)
        def _(i):
            o = pl.multiple_of(i * step, step)
            dst[pl.ds(pl.multiple_of(dst_row + o, step), step), :] = src[pl.ds(o, step), :]

    for a in range(2):
        put(wts.at[a], fs * blk, own_w[a], blk)
    for a in range(3):
        put(tok.at[a], tp * rows_dev, own_t[a], rows_dev)

    tile = math.gcd(width, 256)

    def multiply(a, w, col, size, clear):
        @pl.loop(0, width // tile)
        def _(j):
            o = pl.ds(pl.multiple_of(j * tile, tile), tile)
            got = jnp.dot(tok[a, :, col], wts[w, size, o], preferred_element_type=F32)
            if clear:
                acc[a, :, o] = got
            else:
                acc[a, :, o] += got

    def use(w, f, clear=False):
        if not aligned:
            return
        o = pl.ds(pl.multiple_of(f * blk, blk), blk)
        for a in ((0, 2) if w == 0 else (1,)):
            multiply(a, w, o, o, clear)

    def hop(s, present, go, compute=True):
        for k in present:
            w_copy(k, s - 1).wait_recv()
            if k in go:
                w_copy(k, s).start()
        if compute:
            for k in present:
                use(arr_of[k], at_ring(pos - sign_of[k] * s))

    def streams(s):
        return (0, 1, 2, 3) if s < half else (0, 1)

    def onward(s):
        return tuple(k for k in range(4) if s < half - (k >= 2))

    hop(1, streams(1), onward(1), compute=False)
    for s in range(1, y_size):
        for a in range(3):
            ty_copy(a, s - 1).wait_recv()
            if s < y_size - 1:
                ty_copy(a, s).start()
            td_copy(a, s).start()
    for s in range(y_size):
        for a in range(3):
            td_copy(a, s).wait_recv()
    for w in range(2):
        use(w, fs, True)
    for k in streams(1):
        use(arr_of[k], at_ring(pos - sign_of[k]))
    if half - 2 > 1:
        @pl.loop(2, half - 1)
        def _(s):
            hop(s, (0, 1, 2, 3), (0, 1, 2, 3))
    if half - 1 > 1:
        hop(half - 1, streams(half - 1), onward(half - 1))
    if half > 1:
        hop(half, streams(half), ())
    if not aligned:
        full = pl.ds(0, depth)
        for a, w in ((0, 0), (1, 1), (2, 0)):
            multiply(a, w, full, full, True)

    step_r = math.gcd(rows, 32)

    @pl.loop(0, rows // step_r)
    def _(i):
        o = pl.ds(pl.multiple_of(i * step_r, step_r), step_r)
        relu = jnp.maximum(acc[0, o, :], 0.0)
        hid[0, o, :] = (2.0 * relu * acc[1, o, :]).astype(BF16)
        hid[1, o, :] = (relu * relu).astype(BF16)

    def term(a, row, size):
        @pl.loop(0, width // tile)
        def _(j):
            o = pl.ds(pl.multiple_of(j * tile, tile), tile)
            grads[a, pl.ds(row, size), o] = lax.dot_general(
                tok[a, :, pl.ds(row, size)], hid[a, :, o], (((0,), (0,)), ((), ())),
                preferred_element_type=F32).astype(BF16)

    def block_term(a, p):
        term(a, pl.multiple_of(at_ring(p) * blk, blk), blk)

    def g_copy(k, s):
        d = half - (k >= 2) - s
        f = at_ring(pos + sign_of[k] * d)
        src = grads.at[arr_of[k], pl.ds(pl.multiple_of(f * blk, blk), blk), :]
        return remote(src, rbuf.at[k, s], g_s.at[k, s], g_r.at[k, s], right if sign_of[k] > 0 else left)

    def add_rows(dst, dst_row, src, count):
        step = math.gcd(count, 32)

        @pl.loop(0, count // step)
        def _(i):
            o = pl.multiple_of(i * step, step)
            at = pl.ds(pl.multiple_of(dst_row + o, step), step)
            dst[at, :] = (dst[at, :].astype(F32) + src[pl.ds(o, step), :].astype(F32)).astype(BF16)

    def g_step(s, which):
        for k in which:
            g_copy(k, s - 1).wait_recv()
            f = at_ring(pos + sign_of[k] * (half - (k >= 2) - s))
            add_rows(grads.at[arr_of[k]], f * blk, rbuf.at[k, s - 1], blk)
            g_copy(k, s).start()

    if not aligned:
        wide = math.gcd(depth, 256)
        for a in range(2):
            @pl.loop(0, depth // wide)
            def _(i):
                term(a, pl.multiple_of(i * wide, wide), wide)
    for k in range(4):
        d = half - (k >= 2)
        if d > 0:
            if aligned:
                block_term(arr_of[k], pos + sign_of[k] * d)
            g_copy(k, 0).start()
    if aligned:
        if half > 1:
            @pl.loop(0, half - 1)
            def _(i):
                d = half - 1 - i
                block_term(0, pos + d)
                block_term(1, pos - d)
        if half > 2:
            @pl.loop(0, half - 2)
            def _(i):
                d = half - 2 - i
                block_term(1, pos + d)
                block_term(0, pos - d)
        for a in range(2):
            block_term(a, pos)

    @pl.loop(0, rows // step_r)
    def _(i):
        o = pl.ds(pl.multiple_of(i * step_r, step_r), step_r)
        relu = jnp.maximum(acc[2, o, :], 0.0)
        hid[2, o, :] = (relu * relu).astype(BF16)

    wide_d = math.gcd(depth, 256)

    def partial(a, h, w):
        @pl.loop(0, depth // wide_d)
        def _(j):
            o = pl.ds(pl.multiple_of(j * wide_d, wide_d), wide_d)
            part[a, :, o] = lax.dot_general(
                hid[h], wts[w, o, :], (((1,), (1,)), ((), ())), preferred_element_type=F32).astype(BF16)

    def prow(yy, cc):
        return pl.multiple_of((yy * 2 + cc) * rows_dev, rows_dev)

    def od_copy(a, yy):
        return remote(part.at[a, pl.ds(prow(yy, 1 - c), rows_dev), :], dbuf.at[a, yy],
                      od_s.at[a, yy], od_r.at[a, yy], mate)

    def oy_copy(a, s):
        t = (y + y_size - 1 - s) % y_size
        return remote(part.at[a, pl.ds(prow(t, c), rows_dev), :], ybuf.at[a, s],
                      oy_s.at[a, s], oy_r.at[a, s], y_next)

    for a, h, w in ((0, 0, 0), (1, 2, 1)):
        partial(a, h, w)
        for yy in range(y_size):
            od_copy(a, yy).start()

    if half > 1:
        g_step(1, onward(1))
    for a in range(2):
        for yy in range(y_size):
            od_copy(a, yy).wait_recv()
            add_rows(part.at[a], prow(yy, c), dbuf.at[a, yy], rows_dev)
        if y_size > 1:
            oy_copy(a, 0).start()
    if half - 1 > 2:
        @pl.loop(2, half - 1)
        def _(s):
            g_step(s, (0, 1, 2, 3))
    for s in range(1, y_size):
        for a in range(2):
            oy_copy(a, s - 1).wait_recv()
            t = (y + y_size - 1 - s) % y_size
            add_rows(part.at[a], prow(t, c), ybuf.at[a, s - 1], rows_dev)
            if s < y_size - 1:
                oy_copy(a, s).start()
    put_own = ((earlier_out, 0), (later_out, 1))
    for out, a in put_own:
        out[...] = part[a, pl.ds(prow(y, c), rows_dev), :]
    if half - 1 >= 2:
        g_step(half - 1, (0, 1))

    ends = [(k, half - 1 - (k >= 2)) for k in range(4)]
    for k, s in ends:
        if s >= 0:
            g_copy(k, s).wait_recv()
    step_b = math.gcd(blk, 32)
    for a, out, tot in ((0, up_out, up_tot_ref), (1, down_out, down_tot_ref)):
        @pl.loop(0, blk // step_b)
        def _(i):
            lo = pl.multiple_of(i * step_b, step_b)
            o = pl.ds(lo, step_b)
            got = grads[a, pl.ds(pl.multiple_of(fs * blk + lo, step_b), step_b), :].astype(F32)
            for k, s in ends:
                if arr_of[k] == a and s >= 0:
                    got += rbuf[k, s, o, :].astype(F32)
            out[o, :] = tot[o, :] + got * factor

    for k in range(4):
        for s in range(half - (k >= 2)):
            w_copy(k, s).wait_send()
            g_copy(k, s).wait_send()
    for a in range(3):
        for s in range(y_size):
            if s < y_size - 1:
                ty_copy(a, s).wait_send()
            td_copy(a, s).wait_send()
    for a in range(2):
        for yy in range(y_size):
            od_copy(a, yy).wait_send()
        for s in range(y_size - 1):
            oy_copy(a, s).wait_send()


def body(n, m, later_rows, earlier_rows, cotangent, up_weight, down_weight, up_total, down_total):
    rows_dev, depth = later_rows.shape
    blk, width = up_weight.shape
    rows, half, y_size = rows_dev * m, n // 2, m // 2
    factor = 1.0 / math.sqrt(rows * n)
    dma = pltpu.SemaphoreType.DMA
    vmem = pl.BlockSpec(memory_space=pltpu.VMEM)
    sums = max(y_size - 1, 1)
    return pl.pallas_call(
        functools.partial(kernel, n, m, factor),
        out_shape=(
            jax.ShapeDtypeStruct((rows_dev, depth), BF16),
            jax.ShapeDtypeStruct((rows_dev, depth), BF16),
            jax.ShapeDtypeStruct((blk, width), F32),
            jax.ShapeDtypeStruct((blk, width), F32),
        ),
        in_specs=[vmem] * 7,
        out_specs=(vmem,) * 4,
        scratch_shapes=[
            pltpu.VMEM((3, rows, depth), BF16),
            pltpu.VMEM((2, depth, width), BF16),
            pltpu.VMEM((3, rows, width), F32),
            pltpu.VMEM((3, rows, width), BF16),
            pltpu.VMEM((2, depth, width), BF16),
            pltpu.VMEM((4, half, blk, width), BF16),
            pltpu.VMEM((2, rows, depth), BF16),
            pltpu.VMEM((2, y_size, rows_dev, depth), BF16),
            pltpu.VMEM((2, sums, rows_dev, depth), BF16),
            dma((3, y_size)), dma((3, y_size)), dma((3, y_size)), dma((3, y_size)),
            dma((4, half)), dma((4, half)), dma((4, half)), dma((4, half)),
            dma((2, y_size)), dma((2, y_size)), dma((2, sums)), dma((2, sums)),
        ],
        compiler_params=pltpu.CompilerParams(
            collective_id=0, has_side_effects=True, vmem_limit_bytes=67043328
        ),
        name="feed_forward_step",
    )(later_rows, earlier_rows, cotangent, up_weight, down_weight, up_total, down_total)


def solution(mesh):
    return jax.shard_map(
        functools.partial(body, mesh.shape["fs"], mesh.shape["tp"]),
        mesh=mesh,
        in_specs=(
            P(("fs", "tp"), None),
            P(("fs", "tp"), None),
            P(("fs", "tp"), None),
            P("fs", "tp"),
            P("fs", "tp"),
            P("fs", "tp"),
            P("fs", "tp"),
        ),
        out_specs=(P(("fs", "tp"), None), P(("fs", "tp"), None), P("fs", "tp"), P("fs", "tp")),
        check_vma=False,
    )
```

time: 489 us -> 187 us (0.38)
  waiting for transfers between devices: 428 us -> 0 us
  Pallas kernels: 0 us -> 180 us
  matrix products: 38.5 us -> 0 us
  between operations: 13.9 us -> 0.65 us
    reduce_scatter x4 -> x0, waiting for transfers between devices: 229 us -> none  [the longest x2 164 us: grad_owner(): lax.psum_scatter(lax.dot_general(group, right, (((0,), (0,)), ((), ())),...]
    all_gather x5 -> x0, waiting for transfers between devices: 195 us -> none  [the longest x1 74.9 us: body(): lax.all_gather(up_weight, 'fs', axis=0, tiled=True)]
    pallas_call x0 -> x1, Pallas kernels: none -> 180 us  [body(): pl.pallas_call(functools.partial(kernel, n, m, factor), out_shape=(jax.Sh...]
    dot_general x6 -> x0, matrix products: 38.5 us -> none  [the longest x2 15.9 us: contract_last(): lax.dot_general(left, right, (((1,), (1,)), ((), ())), preferred_element_...]
  transfers between devices with their start and end apart: 9 -> 0, of which waited for: 9 -> 0; matrix products, arithmetic and copies ran while one was open for 9% -> 0% of each run, Pallas kernels for 0% -> 0%
where the time goes in v1:
time: 187 us
  Pallas kernels  180 us (96%)
  local copies, waits for them, and re-layouts  6.43 us (3%)
    pallas_call x1, Pallas kernels, body(): pl.pallas_call(functools.partial(kernel, n, m, factor), out_shape=(jax.Sh...  180 us
    unnamed x8, local copies, waits for them, and re-layouts  6.43 us

profile of v1, /device:TPU:0, one launch (start us, length us, event | category | flops | bytes accessed | tf_op | source)
XLA Modules:
  0.0 187.0 jit_solution(5801476849139756608)
XLA Ops:
  0.6 179.9 %feed_forward_step.1 = (bf16[128,2048]{1,0:T(8,128)(2,1)}, bf16[128,2048]{1,0:T(8,128)(2,1)}, f32[256,1024]{1,0:T(8,128)}, f32[256,1024]{1,0:T(8,128)}) custom-call(bf16[128,2048]{1,0:T(8,128)(2,1)} %later_ref.1, bf16[128,2048]{1,0:T(8,128)(2,1)} %earlier_ref.1, bf16[128,2048]{1,0:T(8,128)(2,1)} %cot_ref.1, bf16[256,1024]{1,0:T(8,128)(2,1)} %up_ref.1, ...), custom_call_target="tpu_custom_call" | custom-call | tf_op jit(solution)/shard_map/feed_forward_step/pallas_call | solution.py:350
  180.6 0.0 copy-start.1
  180.6 2.0 %copy.15 = bf16[128,2048]{1,0:T(8,128)(2,1)} copy(bf16[128,2048]{1,0:T(8,128)(2,1)} %get-tuple-element.8) | data formatting | bytes 1048576
  182.6 1.9 %copy.16 = bf16[128,2048]{1,0:T(8,128)(2,1)} copy(bf16[128,2048]{1,0:T(8,128)(2,1)} %get-tuple-element.9) | data formatting | bytes 1048576
  184.4 0.0 copy-done.1
  184.4 0.0 copy-start
  184.4 1.0 copy.17
  185.4 0.6 copy-done
  186.1 1.0 copy.18
Async XLA Ops:
  180.6 3.9 %copy-start.1 = (f32[256,1024]{1,0:T(8,128)S(1)}, f32[256,1024]{1,0:T(8,128)}, u32[]{:S(2)}) copy-start(f32[256,1024]{1,0:T(8,128)} %get-tuple-element.10) | copy-start | bytes 3145732
  184.4 1.6 copy-start

commit v2 on v1

--- a/solution.py
+++ b/solution.py
@@ -41,8 +41,8 @@
     return jnp.where(x == 0, z_size * wide + z_size - 1 - z, z * wide + r)
 
 
-def kernel(n, m, factor,
-           later_ref, earlier_ref, cot_ref, up_ref, down_ref, up_tot_ref, down_tot_ref,
+def kernel(n, m, parts,
+           later_ref, earlier_ref, cot_ref, up_ref, down_ref,
            later_out, earlier_out, up_out, down_out,
            tok, wts, acc, hid, grads, rbuf, part, dbuf, ybuf,
            ty_s, ty_r, td_s, td_r, w_s, w_r, g_s, g_r, od_s, od_r, oy_s, oy_r):
@@ -51,6 +51,7 @@
     rows = rows_dev * m
     half, y_size = n // 2, m // 2
     aligned = blk % 128 == 0
+    wide_q = width // parts
     fs, tp = lax.axis_index("fs"), lax.axis_index("tp")
     x_size = columns_of(n)
     pos = fs_to_ring(fs, n, x_size)
@@ -74,9 +75,6 @@
         return pltpu.make_async_remote_copy(
             src_ref=src, dst_ref=dst, send_sem=send, recv_sem=recv, device_id=to, device_id_type=MESH)
 
-    def wrows(a, f):
-        return wts.at[a, pl.ds(pl.multiple_of(f * blk, blk), blk), :]
-
     def trows(a, t):
         return tok.at[a, pl.ds(pl.multiple_of(t * rows_dev, rows_dev), rows_dev), :]
 
@@ -84,10 +82,14 @@
 
     arr_of, sign_of = (0, 1, 1, 0), (1, -1, 1, -1)
 
-    def w_copy(k, s, first=False):
+    def cut(q):
+        return pl.ds(q * wide_q, wide_q)
+
+    def w_copy(k, s, q, first=False):
         f = at_ring(pos - sign_of[k] * s)
-        src = own_w[arr_of[k]] if first else wrows(arr_of[k], f)
-        return remote(src, wrows(arr_of[k], f), w_s.at[k, s], w_r.at[k, s], right if sign_of[k] > 0 else left)
+        there = wts.at[arr_of[k], pl.ds(pl.multiple_of(f * blk, blk), blk), cut(q)]
+        src = own_w[arr_of[k]].at[:, cut(q)] if first else there
+        return remote(src, there, w_s.at[k, s, q], w_r.at[k, s, q], right if sign_of[k] > 0 else left)
 
     def ty_copy(a, s, first=False):
         t = ((y + y_size - s) % y_size) * 2 + c
@@ -97,9 +99,10 @@
         t = ((y + y_size - s) % y_size) * 2 + c
         return remote(own_t[a] if first else trows(a, t), trows(a, t), td_s.at[a, s], td_r.at[a, s], mate)
 
-    for k in range(4):
-        if half - (k >= 2) > 0:
-            w_copy(k, 0, True).start()
+    every = tuple((k, q) for pair in ((0, 1), (2, 3)) for q in range(parts) for k in pair)
+    longs = tuple((k, q) for k, q in every if k < 2)
+    for k, q in every:
+        w_copy(k, 0, q, True).start()
     for a in range(3):
         if y_size > 1:
             ty_copy(a, 0, True).start()
@@ -119,41 +122,38 @@
     for a in range(3):
         put(tok.at[a], tp * rows_dev, own_t[a], rows_dev)
 
-    tile = math.gcd(width, 256)
-
-    def multiply(a, w, col, size, clear):
-        @pl.loop(0, width // tile)
+    tile = math.gcd(wide_q, 256)
+
+    def multiply(a, w, rows_w, clear, q=None):
+        first, count = (0, width) if q is None else (q * wide_q, wide_q)
+
+        @pl.loop(0, count // tile)
         def _(j):
-            o = pl.ds(pl.multiple_of(j * tile, tile), tile)
-            got = jnp.dot(tok[a, :, col], wts[w, size, o], preferred_element_type=F32)
+            o = pl.ds(pl.multiple_of(first + j * tile, tile), tile)
+            got = jnp.dot(tok[a, :, rows_w], wts[w, rows_w, o], preferred_element_type=F32)
             if clear:
                 acc[a, :, o] = got
             else:
                 acc[a, :, o] += got
 
-    def use(w, f, clear=False):
+    def use(w, f, clear=False, q=None):
         if not aligned:
             return
         o = pl.ds(pl.multiple_of(f * blk, blk), blk)
         for a in ((0, 2) if w == 0 else (1,)):
-            multiply(a, w, o, o, clear)
-
-    def hop(s, present, go, compute=True):
-        for k in present:
-            w_copy(k, s - 1).wait_recv()
-            if k in go:
-                w_copy(k, s).start()
-        if compute:
-            for k in present:
-                use(arr_of[k], at_ring(pos - sign_of[k] * s))
-
-    def streams(s):
-        return (0, 1, 2, 3) if s < half else (0, 1)
-
-    def onward(s):
-        return tuple(k for k in range(4) if s < half - (k >= 2))
-
-    hop(1, streams(1), onward(1), compute=False)
+            multiply(a, w, o, clear, q)
+
+    def forward(s, present, go):
+        for k, q in present:
+            w_copy(k, s - 1, q).wait_recv()
+            if (k, q) in go:
+                w_copy(k, s, q).start()
+
+    def use_step(s):
+        for k in range(4):
+            use(arr_of[k], at_ring(pos - sign_of[k] * s))
+
+    forward(1, every, every if half > 2 else longs)
     for s in range(1, y_size):
         for a in range(3):
             ty_copy(a, s - 1).wait_recv()
@@ -165,75 +165,87 @@
             td_copy(a, s).wait_recv()
     for w in range(2):
         use(w, fs, True)
-    for k in streams(1):
-        use(arr_of[k], at_ring(pos - sign_of[k]))
-    if half - 2 > 1:
+    if half > 3:
         @pl.loop(2, half - 1)
         def _(s):
-            hop(s, (0, 1, 2, 3), (0, 1, 2, 3))
-    if half - 1 > 1:
-        hop(half - 1, streams(half - 1), onward(half - 1))
-    if half > 1:
-        hop(half, streams(half), ())
-    if not aligned:
-        full = pl.ds(0, depth)
-        for a, w in ((0, 0), (1, 1), (2, 0)):
-            multiply(a, w, full, full, True)
+            forward(s, every, every)
+            use_step(s - 1)
+    if half > 2:
+        forward(half - 1, every, longs)
+        use_step(half - 2)
+    use_step(half - 1)
 
     step_r = math.gcd(rows, 32)
 
-    @pl.loop(0, rows // step_r)
-    def _(i):
-        o = pl.ds(pl.multiple_of(i * step_r, step_r), step_r)
-        relu = jnp.maximum(acc[0, o, :], 0.0)
-        hid[0, o, :] = (2.0 * relu * acc[1, o, :]).astype(BF16)
-        hid[1, o, :] = (relu * relu).astype(BF16)
-
-    def term(a, row, size):
-        @pl.loop(0, width // tile)
+    def activate(q):
+        @pl.loop(0, rows // step_r)
+        def _(i):
+            o = pl.ds(pl.multiple_of(i * step_r, step_r), step_r)
+            relu = jnp.maximum(acc[0, o, cut(q)], 0.0)
+            hid[0, o, cut(q)] = (2.0 * relu * acc[1, o, cut(q)]).astype(BF16)
+            hid[1, o, cut(q)] = (relu * relu).astype(BF16)
+
+    def term(a, row, size, q=None):
+        first, count = (0, width) if q is None else (q * wide_q, wide_q)
+
+        @pl.loop(0, count // tile)
         def _(j):
-            o = pl.ds(pl.multiple_of(j * tile, tile), tile)
+            o = pl.ds(pl.multiple_of(first + j * tile, tile), tile)
             grads[a, pl.ds(row, size), o] = lax.dot_general(
                 tok[a, :, pl.ds(row, size)], hid[a, :, o], (((0,), (0,)), ((), ())),
                 preferred_element_type=F32).astype(BF16)
 
-    def block_term(a, p):
-        term(a, pl.multiple_of(at_ring(p) * blk, blk), blk)
-
-    def g_copy(k, s):
+    def block_term(a, p, q=None):
+        term(a, pl.multiple_of(at_ring(p) * blk, blk), blk, q)
+
+    def g_copy(k, s, q):
         d = half - (k >= 2) - s
         f = at_ring(pos + sign_of[k] * d)
-        src = grads.at[arr_of[k], pl.ds(pl.multiple_of(f * blk, blk), blk), :]
-        return remote(src, rbuf.at[k, s], g_s.at[k, s], g_r.at[k, s], right if sign_of[k] > 0 else left)
-
-    def add_rows(dst, dst_row, src, count):
+        src = grads.at[arr_of[k], pl.ds(pl.multiple_of(f * blk, blk), blk), cut(q)]
+        return remote(src, rbuf.at[k, s, :, cut(q)], g_s.at[k, s, q], g_r.at[k, s, q],
+                      right if sign_of[k] > 0 else left)
+
+    def add_rows(dst, dst_row, src, count, columns=slice(None)):
         step = math.gcd(count, 32)
 
         @pl.loop(0, count // step)
         def _(i):
             o = pl.multiple_of(i * step, step)
             at = pl.ds(pl.multiple_of(dst_row + o, step), step)
-            dst[at, :] = (dst[at, :].astype(F32) + src[pl.ds(o, step), :].astype(F32)).astype(BF16)
+            total = dst[at, columns].astype(F32) + src[pl.ds(o, step), columns].astype(F32)
+            dst[at, columns] = total.astype(BF16)
 
     def g_step(s, which):
-        for k in which:
-            g_copy(k, s - 1).wait_recv()
+        for k, q in which:
+            g_copy(k, s - 1, q).wait_recv()
             f = at_ring(pos + sign_of[k] * (half - (k >= 2) - s))
-            add_rows(grads.at[arr_of[k]], f * blk, rbuf.at[k, s - 1], blk)
-            g_copy(k, s).start()
-
-    if not aligned:
-        wide = math.gcd(depth, 256)
-        for a in range(2):
-            @pl.loop(0, depth // wide)
-            def _(i):
-                term(a, pl.multiple_of(i * wide, wide), wide)
-    for k in range(4):
-        d = half - (k >= 2)
-        if d > 0:
+            add_rows(grads.at[arr_of[k]], f * blk, rbuf.at[k, s - 1], blk, cut(q))
+            g_copy(k, s, q).start()
+
+    wide = math.gcd(depth, 256)
+    for q in range(parts):
+        for k in (0, 1):
+            w_copy(k, half - 1, q).wait_recv()
+            use(arr_of[k], at_ring(pos - sign_of[k] * half), q=q)
+        if not aligned:
+            full = pl.ds(0, depth)
+            for a, w in ((0, 0), (1, 1), (2, 0)):
+                multiply(a, w, full, True, q)
+        activate(q)
+        if not aligned:
+            for a in range(2):
+                @pl.loop(0, depth // wide)
+                def _(i):
+                    term(a, pl.multiple_of(i * wide, wide), wide, q)
+        for k in (0, 1):
             if aligned:
-                block_term(arr_of[k], pos + sign_of[k] * d)
-            g_copy(k, 0).start()
+                block_term(arr_of[k], pos + sign_of[k] * half, q)
+            g_copy(k, 0, q).start()
+    for k in (2, 3):
+        if aligned:
+            block_term(arr_of[k], pos + sign_of[k] * (half - 1))
+        for q in range(parts):
+            g_copy(k, 0, q).start()
     if aligned:
         if half > 1:
             @pl.loop(0, half - 1)
@@ -277,13 +289,14 @@
         return remote(part.at[a, pl.ds(prow(t, c), rows_dev), :], ybuf.at[a, s],
                       oy_s.at[a, s], oy_r.at[a, s], y_next)
 
-    for a, h, w in ((0, 0, 0), (1, 2, 1)):
+    def send_partial(a, h, w):
         partial(a, h, w)
         for yy in range(y_size):
             od_copy(a, yy).start()
 
-    if half > 1:
-        g_step(1, onward(1))
+    send_partial(0, 0, 0)
+    g_step(1, every if half > 2 else longs)
+    send_partial(1, 2, 1)
     for a in range(2):
         for yy in range(y_size):
             od_copy(a, yy).wait_recv()
@@ -293,7 +306,7 @@
     if half - 1 > 2:
         @pl.loop(2, half - 1)
         def _(s):
-            g_step(s, (0, 1, 2, 3))
+            g_step(s, every)
     for s in range(1, y_size):
         for a in range(2):
             oy_copy(a, s - 1).wait_recv()
@@ -305,28 +318,27 @@
     for out, a in put_own:
         out[...] = part[a, pl.ds(prow(y, c), rows_dev), :]
     if half - 1 >= 2:
-        g_step(half - 1, (0, 1))
+        g_step(half - 1, longs)
 
     ends = [(k, half - 1 - (k >= 2)) for k in range(4)]
-    for k, s in ends:
-        if s >= 0:
-            g_copy(k, s).wait_recv()
+    for k, q in tuple((k, q) for k, q in every if k >= 2) + longs:
+        g_copy(k, ends[k][1], q).wait_recv()
     step_b = math.gcd(blk, 32)
-    for a, out, tot in ((0, up_out, up_tot_ref), (1, down_out, down_tot_ref)):
+    for a, out in ((0, up_out), (1, down_out)):
         @pl.loop(0, blk // step_b)
         def _(i):
             lo = pl.multiple_of(i * step_b, step_b)
             o = pl.ds(lo, step_b)
             got = grads[a, pl.ds(pl.multiple_of(fs * blk + lo, step_b), step_b), :].astype(F32)
             for k, s in ends:
-                if arr_of[k] == a and s >= 0:
+                if arr_of[k] == a:
                     got += rbuf[k, s, o, :].astype(F32)
-            out[o, :] = tot[o, :] + got * factor
-
-    for k in range(4):
+            out[o, :] = got.astype(BF16)
+
+    for k, q in every:
         for s in range(half - (k >= 2)):
-            w_copy(k, s).wait_send()
-            g_copy(k, s).wait_send()
+            w_copy(k, s, q).wait_send()
+            g_copy(k, s, q).wait_send()
     for a in range(3):
         for s in range(y_size):
             if s < y_size - 1:
@@ -347,15 +359,16 @@
     dma = pltpu.SemaphoreType.DMA
     vmem = pl.BlockSpec(memory_space=pltpu.VMEM)
     sums = max(y_size - 1, 1)
-    return pl.pallas_call(
-        functools.partial(kernel, n, m, factor),
+    parts = 2 if width % 256 == 0 else 1
+    later_out, earlier_grad, up_term, down_term = pl.pallas_call(
+        functools.partial(kernel, n, m, parts),
         out_shape=(
             jax.ShapeDtypeStruct((rows_dev, depth), BF16),
             jax.ShapeDtypeStruct((rows_dev, depth), BF16),
-            jax.ShapeDtypeStruct((blk, width), F32),
-            jax.ShapeDtypeStruct((blk, width), F32),
+            jax.ShapeDtypeStruct((blk, width), BF16),
+            jax.ShapeDtypeStruct((blk, width), BF16),
         ),
-        in_specs=[vmem] * 7,
+        in_specs=[vmem] * 5,
         out_specs=(vmem,) * 4,
         scratch_shapes=[
             pltpu.VMEM((3, rows, depth), BF16),
@@ -368,14 +381,17 @@
             pltpu.VMEM((2, y_size, rows_dev, depth), BF16),
             pltpu.VMEM((2, sums, rows_dev, depth), BF16),
             dma((3, y_size)), dma((3, y_size)), dma((3, y_size)), dma((3, y_size)),
-            dma((4, half)), dma((4, half)), dma((4, half)), dma((4, half)),
+            *[dma((4, half, parts))] * 4,
             dma((2, y_size)), dma((2, y_size)), dma((2, sums)), dma((2, sums)),
         ],
         compiler_params=pltpu.CompilerParams(
             collective_id=0, has_side_effects=True, vmem_limit_bytes=67043328
         ),
         name="feed_forward_step",
-    )(later_rows, earlier_rows, cotangent, up_weight, down_weight, up_total, down_total)
+    )(later_rows, earlier_rows, cotangent, up_weight, down_weight)
+    up_updated = up_total + up_term.astype(F32) * factor
+    down_updated = down_total + down_term.astype(F32) * factor
+    return later_out, earlier_grad, up_updated, down_updated
 
 
 def solution(mesh):

time: 187 us -> 181 us (0.968)
  Pallas kernels: 180 us -> 174 us
  local copies, waits for them, and re-layouts: 6.43 us -> 2.03 us
  other arithmetic: 0 us -> 3.68 us
    pallas_call x1, Pallas kernels: 180 us -> 174 us  [body(): pl.pallas_call(functools.partial(kernel, n, m, parts), out_shape=(jax.Sha...]
    unnamed x8 -> x6, local copies, waits for them, and re-layouts: 6.43 us -> 2.03 us
    add x0 -> x1, other arithmetic: none -> 3.68 us  [body(): down_updated = down_total + down_term.astype(F32) * factor]
where the time goes in v2:
time: 181 us
  Pallas kernels  174 us (96%)
  other arithmetic  3.68 us (2%)
  local copies, waits for them, and re-layouts  2.03 us (1%)
    pallas_call x1, Pallas kernels, body(): pl.pallas_call(functools.partial(kernel, n, m, parts), out_shape=(jax.Sha...  174 us
    add x1, other arithmetic, body(): down_updated = down_total + down_term.astype(F32) * factor  3.68 us

profile of v2, /device:TPU:0, one launch (start us, length us, event | category | flops | bytes accessed | tf_op | source)
XLA Modules:
  0.0 180.5 jit_solution(12887519513331900022)
XLA Ops:
  0.6 174.2 %feed_forward_step.1 = (bf16[128,2048]{1,0:T(8,128)(2,1)}, bf16[128,2048]{1,0:T(8,128)(2,1)}, bf16[256,1024]{1,0:T(8,128)(2,1)}, bf16[256,1024]{1,0:T(8,128)(2,1)}) custom-call(bf16[128,2048]{1,0:T(8,128)(2,1)} %later_ref.1, bf16[128,2048]{1,0:T(8,128)(2,1)} %earlier_ref.1, bf16[128,2048]{1,0:T(8,128)(2,1)} %cot_ref.1, bf16[256,1024]{1,0:T(8,128)(2,1)} %up_ref.1, ...), custom_call_target="tpu_custom_call" | custom-call | tf_op jit(solution)/shard_map/feed_forward_step/pallas_call | solution.py:363
  174.8 0.0 copy-start.1
  174.8 3.7 %multiply_add_fusion = (f32[256,1024]{1,0:T(8,128)}, f32[256,1024]{1,0:T(8,128)}) fusion(f32[256,1024]{1,0:T(8,128)} %param.13, bf16[256,1024]{1,0:T(8,128)(2,1)} %get-tuple-element.11, f32[256,1024]{1,0:T(8,128)} %param.12, bf16[256,1024]{1,0:T(8,128)(2,1)} %get-tuple-element.10), kind=kLoop, calls=%fused_computation | loop fusion | flops 1572864 | bytes 5242880 | tf_op jit(solution)/shard_map/add | solution.py:393
  178.5 0.0 copy-done.1
  178.5 0.0 copy-start
  178.5 0.8 copy.13
  179.3 0.4 copy-done
  179.7 0.8 copy.14
Async XLA Ops:
  174.8 3.7 %copy-start.1 = (bf16[128,2048]{1,0:T(8,128)(2,1)S(1)}, bf16[128,2048]{1,0:T(8,128)(2,1)}, u32[]{:S(2)}) copy-start(bf16[128,2048]{1,0:T(8,128)(2,1)} %get-tuple-element.18) | copy-start | bytes 1572868
  178.5 1.2 copy-start
